TPU v7x, 32 devices: a whole 2x2x4 slice. The times are simulated.
32 devices in a mesh: sp: 4 (over z), fs: 4 (over y, x), tp: 2 (over core).
Axes of the slice: x: 2, y: 2, z: 4, core: 2. Of those that a mesh axis runs over, the one named last changes fastest.
Arguments:
- stream: bfloat16 [4, 1024, 2048], P('fs', 'sp'), may hold values from -6 to 6
- norm_gain: bfloat16 [2048], replicated, may hold values from 0.099609375 to 1.8984375
- query_weight: bfloat16 [2048, 1024], P(None, 'tp'), may hold values from -0.125 to 0.125
- key_weight: bfloat16 [2048, 1024], P(None, 'tp'), may hold values from -0.125 to 0.125
- value_weight: bfloat16 [2048, 1024], P(None, 'tp'), may hold values from -0.125 to 0.125
- filter_input: bfloat16 [2048, 1024], P(None, 'tp'), may hold values from -0.125 to 0.125
- filter_gate: bfloat16 [2048, 1024], P(None, 'tp'), may hold values from -0.125 to 0.125
- score_offset: bfloat16 [4, 1024, 16], P('fs', 'sp', 'tp'), may hold values from -16 to 0
- head_gain: bfloat16 [1024], P('tp'), may hold values from 0.099609375 to 1.8984375
- filter_taps: bfloat16 [31, 1024], P(None, 'tp'), may hold values from -5 to 5
- channel_gain: bfloat16 [1024], P('tp'), may hold values from 0.099609375 to 1.8984375
- channel_shift: bfloat16 [1024], P('tp'), may hold values from -3 to 3
- attend_out: bfloat16 [1024, 2048], P('tp'), may hold values from -0.125 to 0.125
- filter_out: bfloat16 [1024, 2048], P('tp'), may hold values from -0.125 to 0.125
Outputs:
- mixed_out: bfloat16 [4, 1024, 2048], P('fs', ('sp', 'tp'))
- mass_log: float32 [4, 1024, 16], P('fs', 'sp', 'tp')
All inputs are finite; a program needn't handle non-finite values.
Results may differ from a plain program's by a relative error of at most 0.015.
Values may be sent and summed in bfloat16 or wider, within the bound.
No kernel may reach another device: no remote copies, remote signals or barrier semaphores. Data moves between devices by JAX's collectives and lax.ppermute only.
A program may use at most 64 MiB of HBM per device.

v0:
```python
import jax
import jax.numpy as jnp
from jax import lax
from jax.sharding import PartitionSpec as P

HEAD_DIM = 64
CONV = 1024


rms_eps = 1e-06
norm_eps = 1e-05
mass_floor = 0.01


def shifted(value, axis, steps):
    count = lax.axis_size(axis)
    first, last = (max(0, -steps), min(count, count - steps))
    return lax.ppermute(value, axis, [(source, source + steps) for source in range(first, last)])


def local(
    stream,
    norm_gain,
    query_weight,
    key_weight,
    value_weight,
    filter_input,
    filter_gate,
    score_offset,
    head_gain,
    filter_taps,
    channel_gain,
    channel_shift,
    attend_out,
    filter_out,
):
    rows_here = stream.shape[1]
    xfloat = stream[0].astype(jnp.float32)
    normed = xfloat * lax.rsqrt(jnp.mean(xfloat * xfloat, axis=-1, keepdims=True) + rms_eps)
    normed = (normed * norm_gain.astype(jnp.float32)).astype(jnp.bfloat16)

    def project(weight):
        return jnp.dot(normed, weight, preferred_element_type=jnp.float32).astype(jnp.bfloat16)

    queries = project(query_weight)
    keys_here = project(key_weight)
    values_here = project(value_weight)
    conv_in = project(filter_input)
    conv_gate = project(filter_gate)
    offsets_here = score_offset[0]
    heads_here = offsets_here.shape[1]
    first_pos = lax.axis_index("sp") * rows_here
    position = first_pos + jnp.arange(rows_here, dtype=jnp.int32)
    qheads = queries.reshape(rows_here, heads_here, HEAD_DIM)

    def absorb(state_now, kblock, vblock, oblock, first_key):
        attended, weight_mass, survive = state_now
        span = kblock.shape[0]
        kblock = kblock.reshape(span, heads_here, HEAD_DIM)
        vblock = vblock.reshape(span, heads_here, HEAD_DIM)
        scores = jnp.einsum(
            "thd,shd->hts", qheads, kblock, preferred_element_type=jnp.float32
        ) * HEAD_DIM ** (-0.5)
        scores = scores + oblock.astype(jnp.float32).T[:, None, :]
        key_pos = first_key + jnp.arange(span, dtype=jnp.int32)
        strict = ((key_pos[None, :] < position[:, None]) & (key_pos[None, :] >= 0))[None]
        losing = jnp.where(strict, jax.nn.log_sigmoid(-scores), 0.0)
        beyond = lax.cumsum(losing, axis=2, reverse=True) - losing + survive[:, :, None]
        weights = jnp.where(strict, jnp.exp(jax.nn.log_sigmoid(scores) + beyond), 0.0)
        weight_mass = weight_mass + jnp.sum(weights, axis=2)
        attended = attended + jnp.einsum(
            "hts,shd->thd", weights.astype(jnp.bfloat16), vblock, preferred_element_type=jnp.float32
        )
        survive = survive + jnp.sum(losing, axis=2)
        return (attended, weight_mass, survive)

    initial = (
        jnp.zeros((rows_here, heads_here, HEAD_DIM), jnp.float32),
        jnp.zeros((heads_here, rows_here), jnp.float32),
        jnp.zeros((heads_here, rows_here), jnp.float32),
    )
    state_now = absorb(initial, keys_here, values_here, offsets_here, first_pos)

    def pass_turn(turn_index, carried):
        state_now, travelling = carried
        travelling = shifted((travelling[0], travelling[1], travelling[2]), "sp", 1)
        first_key = first_pos - (turn_index + 1) * rows_here
        state_now = absorb(state_now, travelling[0], travelling[1], travelling[2], first_key)
        return (state_now, travelling)

    state_now, travelling = lax.fori_loop(
        0, lax.axis_size("sp") - 1, pass_turn, (state_now, (keys_here, values_here, offsets_here))
    )
    attended, weight_mass, survive = state_now
    head_scale = lax.rsqrt(jnp.mean(attended * attended, axis=-1, keepdims=True) + rms_eps)
    heads_flat = attended * head_scale * head_gain.astype(jnp.float32).reshape(heads_here, HEAD_DIM)
    heads_flat = heads_flat.astype(jnp.bfloat16).reshape(rows_here, heads_here * HEAD_DIM)
    mass_log = jnp.log(jnp.maximum(weight_mass.T, mass_floor))
    gated_rows = (
        conv_in.astype(jnp.float32) * jax.nn.sigmoid(conv_gate.astype(jnp.float32))
    ).astype(jnp.bfloat16)
    reach_back = filter_taps.shape[0] - 1
    earlier = shifted(gated_rows[rows_here - reach_back :], "sp", 1)
    extended = jnp.concatenate([earlier, gated_rows], axis=0).astype(jnp.float32)
    tap_values = filter_taps.astype(jnp.float32)
    filtered = jnp.zeros((rows_here, gated_rows.shape[1]), jnp.float32)
    for tap_index in range(reach_back + 1):
        filtered = filtered + extended[tap_index : tap_index + rows_here] * tap_values[tap_index]
    center = lax.psum(jnp.sum(filtered, axis=-1), "tp") / CONV
    deviation = filtered - center[:, None]
    spread = lax.psum(jnp.sum(deviation * deviation, axis=-1), "tp") / CONV
    conv_out = jax.nn.silu(
        deviation * lax.rsqrt(spread[:, None] + norm_eps) * channel_gain.astype(jnp.float32)
        + channel_shift.astype(jnp.float32)
    ).astype(jnp.bfloat16)
    mixed_out = lax.psum_scatter(
        (
            jnp.dot(heads_flat, attend_out, preferred_element_type=jnp.float32)
            + jnp.dot(conv_out, filter_out, preferred_element_type=jnp.float32)
        ).astype(jnp.bfloat16),
        "tp",
        scatter_dimension=0,
        tiled=True,
    )
    return (mixed_out[None], mass_log[None])


def solution(mesh):
    return jax.shard_map(
        local,
        mesh=mesh,
        in_specs=(
            P("fs", "sp", None),
            P(),
            P(None, "tp"),
            P(None, "tp"),
            P(None, "tp"),
            P(None, "tp"),
            P(None, "tp"),
            P("fs", "sp", "tp"),
            P("tp"),
            P(None, "tp"),
            P("tp"),
            P("tp"),
            P("tp", None),
            P("tp", None),
        ),
        out_specs=(P("fs", ("sp", "tp"), None), P("fs", "sp", "tp")),
        check_vma=False,
    )
```

profile of v0, /device:TPU:27, one launch (start us, length us, event | category | flops | bytes accessed | tf_op | source)
XLA Modules:
  0.0 149.9 jit_solution(6098142235534850311)
XLA Ops:
  7.2 0.8 copy.72
  8.1 0.7 convert_element_type.76
  8.7 1.5 %fusion.15 = f32[256]{0:T(256)S(1)} fusion(bf16[1,256,2048]{2,1,0:T(8,128)(2,1)} %param.16), kind=kLoop, calls=%fused_computation.32 | loop fusion | flops 1572608 | bytes 1049600 | tf_op jit(solution)/shard_map/reduce_sum | solution.py:39
  10.3 2.9 %fusion.31 = f32[256,512]{1,0:T(8,128)S(1)} fusion(bf16[2048,512]{1,0:T(8,128)(2,1)} %param.22, bf16[1,256,2048]{2,1,0:T(8,128)(2,1)} %param.16, f32[2048]{0:T(1024)S(1)} %convert_element_type.76, f32[256]{0:T(256)S(1)} %add_rsqrt_fusion.2), kind=kOutput, calls=%fused_computation.59 | convolution fusion | flops 539623424 | bytes 3679232 | tf_op jit(solution)/shard_map/dot_general | solution.py:43
  13.2 0.8 fusion.26
  14.0 0.7 copy-done.2
  14.7 1.3 collective-permute-start.3
  16.0 2.3 %convolution_convert_fusion.3 = bf16[256,512]{1,0:T(8,128)(2,1)S(1)} fusion(bf16[2048,512]{1,0:T(8,128)(2,1)} %param.18, bf16[1,256,2048]{2,1,0:T(8,128)(2,1)S(1)} %copy-done.1, f32[2048]{0:T(1024)S(1)} %convert_element_type.76, f32[256]{0:T(256)S(1)} %add_rsqrt_fusion.2), kind=kOutput, calls=%fused_computation.50 | convolution fusion | flops 539099136 | bytes 3417088 | tf_op jit(solution)/shard_map/dot_general | solution.py:43
  18.4 0.8 copy.32
  19.2 2.3 %convolution_convert_fusion.2 = bf16[256,512]{1,0:T(8,128)(2,1)S(1)} fusion(bf16[2048,512]{1,0:T(8,128)(2,1)} %param.19, bf16[1,256,2048]{2,1,0:T(8,128)(2,1)S(1)} %copy-done.1, f32[2048]{0:T(1024)S(1)} %convert_element_type.76, f32[256]{0:T(256)S(1)} %add_rsqrt_fusion.2), kind=kOutput, calls=%fused_computation.49 | convolution fusion | flops 539099136 | bytes 3417088 | tf_op jit(solution)/shard_map/dot_general | solution.py:43
  21.6 0.9 copy.33
  22.6 1.7 %fusion.33 = (u8[256,256]{0,1:T(8,128)(4,1)S(1)}, f32[8,256,256]{1,2,0:T(8,128)S(1)}) fusion(f32[8,256]{1,0:T(8,128)S(1)} %convert_bitcast_fusion.1, bf16[256,8,64]{0,2,1:T(8,128)(2,1)} %bitcast.3, bf16[256,8,64]{0,2,1:T(8,128)(2,1)} %bitcast.4), kind=kOutput, calls=%fused_computation.62 | convolution fusion | flops 70713344 | bytes 2695168 | tf_op jit(solution)/shard_map/thd,shd->hts/dot_general | solution.py:61
  24.3 1.4 fusion.71
  25.7 5.1 %fusion.22 = f32[8,256,2,128]{1,0,3,2:T(8,128)S(1)} fusion(f32[8,256,2,128]{1,3,2,0:T(8,128)S(1)} %bitcast.121), kind=kOutput, calls=%fused_computation.42 | output fusion | flops 66584576 | bytes 4194304 | tf_op jit(solution)/shard_map/reduce-window
  30.9 0.1 broadcast_add_fusion.1
  31.0 0.7 copy.35
  31.7 4.0 %fusion.81 = (f32[8,256]{1,0:T(8,128)S(1)}, bf16[8,256,256]{1,2,0:T(8,128)(2,1)}) fusion(f32[8,256,256]{1,2,0:T(8,128)S(1)} %get-tuple-element.299, u8[256,256]{0,1:T(8,128)(4,1)S(1)} %get-tuple-element.298, f32[8,256,2,128]{1,3,2,0:T(8,128)S(1)} %copy.35, pred[256,256]{0,1:T(8,128)(4,1)S(1)} %compare_and_fusion.1), kind=kLoop, calls=%fused_computation.149 | loop fusion | flops 12580864 | bytes 5382144 | tf_op jit(solution)/shard_map/reduce_sum | solution.py:70
  35.7 0.8 convolution_convert_fusion.4
  36.6 1.5 %convolution_bitcast_fusion.1 = f32[256,8,64]{0,2,1:T(8,128)S(1)} fusion(bf16[256,8,64]{0,2,1:T(8,128)(2,1)S(1)} %bitcast.124, bf16[8,256,256]{1,2,0:T(8,128)(2,1)} %get-tuple-element.260), kind=kOutput, calls=%fused_computation.46 | convolution fusion | flops 67108864 | bytes 1835008 | tf_op jit(solution)/shard_map/hts,shd->thd/dot_general | solution.py:71
  38.2 72.5 %while.25 = (s32[]{:T(128)}, f32[256,8,64]{0,2,1:T(8,128)S(1)}, f32[8,256]{1,0:T(8,128)S(1)}, f32[8,256]{1,0:T(8,128)S(1)}, bf16[256,512]{0,1:T(8,128)(2,1)}, /*...) while((s32[]{:T(128)}, f32[256,8,64]{0,2,1:T(8,128)S(1)}, ...), condition=%wide.region_10.11_spmd.clone.clone, body=%wide.region_5.10_spmd.clone.clone.sunk | while | flops 226698240 | bytes 30769928 | solution.py:91
  38.4 1.3 collective-permute-start.1
  39.7 1.3 collective-permute-start.2
  41.0 1.3 collective-permute-start
  42.5 0.9 collective-permute-done.1
  43.4 6.9 %collective-permute-done.2 = bf16[256,512]{0,1:T(8,128)(2,1)S(1)} collective-permute-done((bf16[256,512]{0,1:T(8,128)(2,1)}, bf16[256,512]{0,1:T(8,128)(2,1)S(1)}, u32[]{:S(2)}, u32[]{:S(2)}) %collective-permute-start.2) | collective-permute-done | bytes 262176 | tf_op jit(solution)/shard_map/while/body/eval_jaxpr/ppermute | solution.py:18
  50.2 1.7 %fusion.118 = (u8[256,256]{0,1:T(8,128)(4,1)S(1)}, f32[8,256,256]{1,2,0:T(8,128)S(1)}) fusion(f32[8,256]{1,0:T(8,128)S(1)} %convert_bitcast_fusion.3, bf16[256,8,64]{0,2,1:T(8,128)(2,1)} %get-tuple-element.401, bf16[256,8,64]{0,2,1:T(8,128)(2,1)S(1)} %bitcast.122), kind=kOutput, calls=%fused_computation.18.clone.1 | convolution fusion | flops 70713344 | bytes 2695168 | tf_op jit(solution)/shard_map/while/body/eval_jaxpr/thd,shd->hts/dot_general | solution.py:61
  51.9 1.6 %fusion.119 = (f32[8,256]{1,0:T(8,128)S(1)}, f32[8,256,256]{1,2,0:T(8,128)S(1)}) fusion(f32[8,256]{1,0:T(8,128)S(1)} %convert_bitcast_fusion.3, f32[8,256,256]{1,2,0:T(8,128)S(1)} %get-tuple-element.366, u8[256,256]{0,1:T(8,128)(4,1)S(1)} %get-tuple-element.365, pred[256,256]{0,1:T(8,128)(4,1)S(1)} %compare_and_fusion.3), kind=kLoop, calls=%fused_computation.26.clone.1 | loop fusion | flops 7337984 | bytes 4341760 | tf_op jit(solution)/shard_map/while/body/eval_jaxpr/reduce_sum | solution.py:74
  53.5 5.1 %fusion.120 = f32[8,256,2,128]{1,0,3,2:T(8,128)S(1)} fusion(f32[8,256,2,128]{1,3,2,0:T(8,128)S(1)} %bitcast.119), kind=kOutput, calls=%fused_computation.10.clone.1 | output fusion | flops 66584576 | bytes 4194304 | tf_op jit(solution)/shard_map/reduce-window.6
  58.8 0.7 copy.48
  59.5 3.6 %fusion.122 = (f32[8,256]{1,0:T(8,128)S(1)}, bf16[8,256,256]{1,2,0:T(8,128)(2,1)S(1)}) fusion(f32[8,256]{1,0:T(8,128)S(1)} %get-tuple-element.385, u8[256,256]{0,1:T(8,128)(4,1)S(1)} %get-tuple-element.365, f32[8,256,2,128]{1,3,2,0:T(8,128)S(1)} %copy.48, f32[8,256]{1,0:T(8,128)S(1)} %convert_bitcast_fusion.3, ...), kind=kLoop, calls=%fused_computation.147.clone.1 | loop fusion | flops 14153728 | bytes 5398528 | tf_op jit(solution)/shard_map/while/body/eval_jaxpr/reduce_sum | solution.py:70
  63.1 0.3 fusion.123
  63.4 0.7 copy.67
  64.2 1.3 collective-permute-start.1
  65.5 1.3 collective-permute-start.2
  66.8 1.3 collective-permute-start
  68.3 0.3 collective-permute-done.1
  68.5 4.9 %collective-permute-done.2 = bf16[256,512]{0,1:T(8,128)(2,1)S(1)} collective-permute-done((bf16[256,512]{0,1:T(8,128)(2,1)}, bf16[256,512]{0,1:T(8,128)(2,1)S(1)}, u32[]{:S(2)}, u32[]{:S(2)}) %collective-permute-start.2) | collective-permute-done | bytes 262176 | tf_op jit(solution)/shard_map/while/body/eval_jaxpr/ppermute | solution.py:18
  73.5 1.7 %fusion.118 = (u8[256,256]{0,1:T(8,128)(4,1)S(1)}, f32[8,256,256]{1,2,0:T(8,128)S(1)}) fusion(f32[8,256]{1,0:T(8,128)S(1)} %convert_bitcast_fusion.3, bf16[256,8,64]{0,2,1:T(8,128)(2,1)} %get-tuple-element.401, bf16[256,8,64]{0,2,1:T(8,128)(2,1)S(1)} %bitcast.122), kind=kOutput, calls=%fused_computation.18.clone.1 | convolution fusion | flops 70713344 | bytes 2695168 | tf_op jit(solution)/shard_map/while/body/eval_jaxpr/thd,shd->hts/dot_general | solution.py:61
  75.2 1.6 %fusion.119 = (f32[8,256]{1,0:T(8,128)S(1)}, f32[8,256,256]{1,2,0:T(8,128)S(1)}) fusion(f32[8,256]{1,0:T(8,128)S(1)} %convert_bitcast_fusion.3, f32[8,256,256]{1,2,0:T(8,128)S(1)} %get-tuple-element.366, u8[256,256]{0,1:T(8,128)(4,1)S(1)} %get-tuple-element.365, pred[256,256]{0,1:T(8,128)(4,1)S(1)} %compare_and_fusion.3), kind=kLoop, calls=%fused_computation.26.clone.1 | loop fusion | flops 7337984 | bytes 4341760 | tf_op jit(solution)/shard_map/while/body/eval_jaxpr/reduce_sum | solution.py:74
  76.8 5.1 %fusion.120 = f32[8,256,2,128]{1,0,3,2:T(8,128)S(1)} fusion(f32[8,256,2,128]{1,3,2,0:T(8,128)S(1)} %bitcast.119), kind=kOutput, calls=%fused_computation.10.clone.1 | output fusion | flops 66584576 | bytes 4194304 | tf_op jit(solution)/shard_map/reduce-window.6
  82.1 0.7 copy.48
  82.8 3.6 %fusion.122 = (f32[8,256]{1,0:T(8,128)S(1)}, bf16[8,256,256]{1,2,0:T(8,128)(2,1)S(1)}) fusion(f32[8,256]{1,0:T(8,128)S(1)} %get-tuple-element.385, u8[256,256]{0,1:T(8,128)(4,1)S(1)} %get-tuple-element.365, f32[8,256,2,128]{1,3,2,0:T(8,128)S(1)} %copy.48, f32[8,256]{1,0:T(8,128)S(1)} %convert_bitcast_fusion.3, ...), kind=kLoop, calls=%fused_computation.147.clone.1 | loop fusion | flops 14153728 | bytes 5398528 | tf_op jit(solution)/shard_map/while/body/eval_jaxpr/reduce_sum | solution.py:70
  86.4 0.3 fusion.123
  86.7 0.7 copy.67
  87.4 1.3 collective-permute-start.1
  88.7 1.3 collective-permute-start.2
  90.0 1.3 collective-permute-start
  91.5 0.3 collective-permute-done.1
  91.8 4.9 %collective-permute-done.2 = bf16[256,512]{0,1:T(8,128)(2,1)S(1)} collective-permute-done((bf16[256,512]{0,1:T(8,128)(2,1)}, bf16[256,512]{0,1:T(8,128)(2,1)S(1)}, u32[]{:S(2)}, u32[]{:S(2)}) %collective-permute-start.2) | collective-permute-done | bytes 262176 | tf_op jit(solution)/shard_map/while/body/eval_jaxpr/ppermute | solution.py:18
  96.7 1.7 %fusion.118 = (u8[256,256]{0,1:T(8,128)(4,1)S(1)}, f32[8,256,256]{1,2,0:T(8,128)S(1)}) fusion(f32[8,256]{1,0:T(8,128)S(1)} %convert_bitcast_fusion.3, bf16[256,8,64]{0,2,1:T(8,128)(2,1)} %get-tuple-element.401, bf16[256,8,64]{0,2,1:T(8,128)(2,1)S(1)} %bitcast.122), kind=kOutput, calls=%fused_computation.18.clone.1 | convolution fusion | flops 70713344 | bytes 2695168 | tf_op jit(solution)/shard_map/while/body/eval_jaxpr/thd,shd->hts/dot_general | solution.py:61
  98.4 1.6 %fusion.119 = (f32[8,256]{1,0:T(8,128)S(1)}, f32[8,256,256]{1,2,0:T(8,128)S(1)}) fusion(f32[8,256]{1,0:T(8,128)S(1)} %convert_bitcast_fusion.3, f32[8,256,256]{1,2,0:T(8,128)S(1)} %get-tuple-element.366, u8[256,256]{0,1:T(8,128)(4,1)S(1)} %get-tuple-element.365, pred[256,256]{0,1:T(8,128)(4,1)S(1)} %compare_and_fusion.3), kind=kLoop, calls=%fused_computation.26.clone.1 | loop fusion | flops 7337984 | bytes 4341760 | tf_op jit(solution)/shard_map/while/body/eval_jaxpr/reduce_sum | solution.py:74
  100.0 5.1 %fusion.120 = f32[8,256,2,128]{1,0,3,2:T(8,128)S(1)} fusion(f32[8,256,2,128]{1,3,2,0:T(8,128)S(1)} %bitcast.119), kind=kOutput, calls=%fused_computation.10.clone.1 | output fusion | flops 66584576 | bytes 4194304 | tf_op jit(solution)/shard_map/reduce-window.6
  105.3 0.7 copy.48
  106.0 3.6 %fusion.122 = (f32[8,256]{1,0:T(8,128)S(1)}, bf16[8,256,256]{1,2,0:T(8,128)(2,1)S(1)}) fusion(f32[8,256]{1,0:T(8,128)S(1)} %get-tuple-element.385, u8[256,256]{0,1:T(8,128)(4,1)S(1)} %get-tuple-element.365, f32[8,256,2,128]{1,3,2,0:T(8,128)S(1)} %copy.48, f32[8,256]{1,0:T(8,128)S(1)} %convert_bitcast_fusion.3, ...), kind=kLoop, calls=%fused_computation.147.clone.1 | loop fusion | flops 14153728 | bytes 5398528 | tf_op jit(solution)/shard_map/while/body/eval_jaxpr/reduce_sum | solution.py:70
  109.6 0.3 fusion.123
  109.9 0.7 copy.67
  111.0 2.1 %fusion.85 = f32[256,2048]{1,0:T(8,128)} fusion(bf16[256,512]{0,1:T(8,128)(2,1)S(1)} %bitcast.123, bf16[512,2048]{1,0:T(8,128)(2,1)S(1)} %copy-done), kind=kOutput, calls=%fused_computation.152 | convolution fusion | flops 536870912 | bytes 4456448 | tf_op jit(solution)/shard_map/dot_general | solution.py:118
  113.3 2.6 %fusion.79 = (f32[256]{0:T(256)S(1)}, f32[256,512]{1,0:T(8,128)S(1)}) fusion(f32[512]{0:T(512)S(1)} %bitcast.156, f32[286,512]{1,0:T(8,128)S(1)} %maximum_convert_fusion, f32[512]{0:T(512)S(1)} %bitcast.155, f32[512]{0:T(512)S(1)} %bitcast.154, f32[512]{0:T(512)S(1)} %bitcast.153, f32[512]{0:T(512)S(1)} %bitcast.152, f32[512]{0:T(512)S(1)} %bitcast.151, ...), kind=kLoop, calls=%fused_computation.148 | loop fusion | flops 8126208 | bytes 16841728 | tf_op jit(solution)/shard_map/reduce_sum | solution.py:109
  115.9 9.6 %psum.14 = f32[256]{0:T(256)S(1)} all-reduce(f32[256]{0:T(256)S(1)} %get-tuple-element.257), channel_id=1, replica_groups=mesh['sp'=4,'fs'=4,'tp'=2] {'tp'}, use_global_device_ids=true, to_apply=%region_13.14 | all-reduce | flops 256 | bytes 2048 | tf_op jit(solution)/shard_map/psum | solution.py:109
  125.5 0.2 multiply_reduce_fusion
  125.7 2.5 %psum.15 = f32[256]{0:T(256)S(1)} all-reduce(f32[256]{0:T(256)S(1)} %multiply_reduce_fusion), channel_id=1, replica_groups=mesh['sp'=4,'fs'=4,'tp'=2] {'tp'}, use_global_device_ids=true, to_apply=%region_15.16 | all-reduce | flops 256 | bytes 2048 | tf_op jit(solution)/shard_map/psum | solution.py:111
  128.2 4.1 %fusion.14 = bf16[256,2048]{1,0:T(8,128)(2,1)} fusion(f32[256,2048]{1,0:T(8,128)} %fusion.85, bf16[512,2048]{1,0:T(8,128)(2,1)} %param.29, f32[256,512]{1,0:T(8,128)S(1)} %get-tuple-element.258, f32[512]{0:T(512)S(1)} %convert_element_type.91, f32[512]{0:T(512)S(1)} %convert_element_type.90, f32[256]{0:T(256)S(1)} %add_rsqrt_fusion.1, ...), kind=kOutput, calls=%fused_computation.31 | convolution fusion | flops 539099136 | bytes 5773312 | tf_op jit(solution)/shard_map/dot_general | solution.py:119
  132.3 0.6 log_bitcast_fusion
  132.9 10.1 %reduce-scatter.2.cloned.1.call-done = bf16[128,2048]{1,0:T(8,128)(2,1)} async-done(((bf16[256,2048]{1,0:T(8,128)(2,1)}), bf16[128,2048]{1,0:T(8,128)(2,1)}) %reduce-scatter.2.cloned.1.call-update) | async-done | bytes 524304 | tf_op jit(solution)/shard_map/reduce_scatter | solution.py:116
  (81 shorter events, 2.0 us)
Async XLA Ops:
  7.2 103.8 %copy-start = (bf16[512,2048]{1,0:T(8,128)(2,1)S(1)}, bf16[512,2048]{1,0:T(8,128)(2,1)}, u32[]{:S(2)}) copy-start(bf16[512,2048]{1,0:T(8,128)(2,1)} %param.28) | copy-start | bytes 6291460
  7.2 135.9 %reduce-scatter.2.cloned.1.call-start = ((), (), s32[]{:S(2)}) async-start(), calls=%async_computation.1 | async-start | bytes 1572864 | tf_op jit(solution)/shard_map/reduce_scatter | solution.py:116
  10.3 2.9 %copy-start.1 = (bf16[1,256,2048]{2,1,0:T(8,128)(2,1)S(1)}, bf16[1,256,2048]{2,1,0:T(8,128)(2,1)}, u32[]{:S(2)}) copy-start(bf16[1,256,2048]{2,1,0:T(8,128)(2,1)} %param.16) | copy-start | bytes 3145732
  10.3 2.9 %copy-start.8 = (bf16[2048,512]{1,0:T(8,128)(2,1)S(1)}, bf16[2048,512]{1,0:T(8,128)(2,1)}, u32[]{:S(2)}) copy-start(bf16[2048,512]{1,0:T(8,128)(2,1)} %param.21) | copy-start | bytes 6291460
  14.0 0.7 copy-start.2
  14.7 98.5 %collective-permute-start.3 = (bf16[30,512]{1,0:T(8,128)(2,1)S(1)}, bf16[30,512]{1,0:T(8,128)(2,1)S(1)}, u32[]{:S(2)}, u32[]{:S(2)}) collective-permute-start(bf16[30,512]{1,0:T(8,128)(2,1)S(1)} %slice.278), channel_id=1, source_target_pairs={{0,8},{8,16},{16,24},{1,9},{9,17},{17,25},{2,10},{10,18},{18,26},{... | collective-permute-start | bytes 92168 | tf_op jit(solution)/shard_map/ppermute | solution.py:18
  31.7 4.0 %copy-start.9 = (bf16[2048,512]{1,0:T(8,128)(2,1)S(1)}, bf16[2048,512]{1,0:T(8,128)(2,1)}, u32[]{:S(2)}) copy-start(bf16[2048,512]{1,0:T(8,128)(2,1)} %param.20) | copy-start | bytes 6291460
  38.2 72.6 %copy-start.5 = (bf16[512]{0:T(512)(128)(2,1)S(1)}, bf16[512]{0:T(512)(128)(2,1)}, u32[]{:S(2)}) copy-start(bf16[512]{0:T(512)(128)(2,1)} %param.24) | copy-start | bytes 3076
  38.2 72.6 %copy-start.4 = (bf16[31,512]{1,0:T(8,128)(2,1)S(1)}, bf16[31,512]{1,0:T(8,128)(2,1)}, u32[]{:S(2)}) copy-start(bf16[31,512]{1,0:T(8,128)(2,1)} %param.25) | copy-start | bytes 95236
  38.4 5.0 %collective-permute-start.1 = (bf16[256,8]{0,1:T(8,128)(2,1)S(1)}, bf16[256,8]{0,1:T(8,128)(2,1)S(1)}, u32[]{:S(2)}, u32[]{:S(2)}) collective-permute-start(bf16[256,8]{0,1:T(8,128)(2,1)S(1)} %get-tuple-element.388), channel_id=1, source_target_pairs={{0,8},{8,16},{16,24},{1,9},{9,17},{17,25},{2,10},{10,18},{18,26},{... | collective-permute-start | bytes 12296 | tf_op jit(solution)/shard_map/while/body/eval_jaxpr/ppermute | solution.py:18
  39.7 10.5 %collective-permute-start.2 = (bf16[256,512]{0,1:T(8,128)(2,1)}, bf16[256,512]{0,1:T(8,128)(2,1)S(1)}, u32[]{:S(2)}, u32[]{:S(2)}) collective-permute-start(bf16[256,512]{0,1:T(8,128)(2,1)} %get-tuple-element.386), channel_id=1, source_target_pairs={{0,8},{8,16},{16,24},{1,9},{9,17},{17,25},{2,10},{10,18},{18,26},{... | collective-permute-start | bytes 786440 | tf_op jit(solution)/shard_map/while/body/eval_jaxpr/ppermute | solution.py:18
  41.0 22.1 %collective-permute-start = (bf16[256,512]{0,1:T(8,128)(2,1)S(1)}, bf16[256,512]{0,1:T(8,128)(2,1)S(1)}, u32[]{:S(2)}, u32[]{:S(2)}) collective-permute-start(bf16[256,512]{0,1:T(8,128)(2,1)S(1)} %get-tuple-element.387), channel_id=1, source_target_pairs={{0,8},{8,16},{16,24},{1,9},{9,17},{17,25},{2,10},{10,18},{18,26},{... | collective-permute-start | bytes 786440 | tf_op jit(solution)/shard_map/while/body/eval_jaxpr/ppermute | solution.py:18
  64.2 4.4 %collective-permute-start.1 = (bf16[256,8]{0,1:T(8,128)(2,1)S(1)}, bf16[256,8]{0,1:T(8,128)(2,1)S(1)}, u32[]{:S(2)}, u32[]{:S(2)}) collective-permute-start(bf16[256,8]{0,1:T(8,128)(2,1)S(1)} %get-tuple-element.388), channel_id=1, source_target_pairs={{0,8},{8,16},{16,24},{1,9},{9,17},{17,25},{2,10},{10,18},{18,26},{... | collective-permute-start | bytes 12296 | tf_op jit(solution)/shard_map/while/body/eval_jaxpr/ppermute | solution.py:18
  65.5 8.0 %collective-permute-start.2 = (bf16[256,512]{0,1:T(8,128)(2,1)}, bf16[256,512]{0,1:T(8,128)(2,1)S(1)}, u32[]{:S(2)}, u32[]{:S(2)}) collective-permute-start(bf16[256,512]{0,1:T(8,128)(2,1)} %get-tuple-element.386), channel_id=1, source_target_pairs={{0,8},{8,16},{16,24},{1,9},{9,17},{17,25},{2,10},{10,18},{18,26},{... | collective-permute-start | bytes 786440 | tf_op jit(solution)/shard_map/while/body/eval_jaxpr/ppermute | solution.py:18
  66.8 19.6 %collective-permute-start = (bf16[256,512]{0,1:T(8,128)(2,1)S(1)}, bf16[256,512]{0,1:T(8,128)(2,1)S(1)}, u32[]{:S(2)}, u32[]{:S(2)}) collective-permute-start(bf16[256,512]{0,1:T(8,128)(2,1)S(1)} %get-tuple-element.387), channel_id=1, source_target_pairs={{0,8},{8,16},{16,24},{1,9},{9,17},{17,25},{2,10},{10,18},{18,26},{... | collective-permute-start | bytes 786440 | tf_op jit(solution)/shard_map/while/body/eval_jaxpr/ppermute | solution.py:18
  87.4 4.4 %collective-permute-start.1 = (bf16[256,8]{0,1:T(8,128)(2,1)S(1)}, bf16[256,8]{0,1:T(8,128)(2,1)S(1)}, u32[]{:S(2)}, u32[]{:S(2)}) collective-permute-start(bf16[256,8]{0,1:T(8,128)(2,1)S(1)} %get-tuple-element.388), channel_id=1, source_target_pairs={{0,8},{8,16},{16,24},{1,9},{9,17},{17,25},{2,10},{10,18},{18,26},{... | collective-permute-start | bytes 12296 | tf_op jit(solution)/shard_map/while/body/eval_jaxpr/ppermute | solution.py:18
  88.7 8.0 %collective-permute-start.2 = (bf16[256,512]{0,1:T(8,128)(2,1)}, bf16[256,512]{0,1:T(8,128)(2,1)S(1)}, u32[]{:S(2)}, u32[]{:S(2)}) collective-permute-start(bf16[256,512]{0,1:T(8,128)(2,1)} %get-tuple-element.386), channel_id=1, source_target_pairs={{0,8},{8,16},{16,24},{1,9},{9,17},{17,25},{2,10},{10,18},{18,26},{... | collective-permute-start | bytes 786440 | tf_op jit(solution)/shard_map/while/body/eval_jaxpr/ppermute | solution.py:18
  90.0 19.5 %collective-permute-start = (bf16[256,512]{0,1:T(8,128)(2,1)S(1)}, bf16[256,512]{0,1:T(8,128)(2,1)S(1)}, u32[]{:S(2)}, u32[]{:S(2)}) collective-permute-start(bf16[256,512]{0,1:T(8,128)(2,1)S(1)} %get-tuple-element.387), channel_id=1, source_target_pairs={{0,8},{8,16},{16,24},{1,9},{9,17},{17,25},{2,10},{10,18},{18,26},{... | collective-permute-start | bytes 786440 | tf_op jit(solution)/shard_map/while/body/eval_jaxpr/ppermute | solution.py:18
  111.0 2.1 %copy-start.6 = (bf16[512]{0:T(512)(128)(2,1)S(1)}, bf16[512]{0:T(512)(128)(2,1)}, u32[]{:S(2)}) copy-start(bf16[512]{0:T(512)(128)(2,1)} %param.26) | copy-start | bytes 3076
  111.0 2.2 %copy-start.7 = (bf16[512]{0:T(512)(128)(2,1)S(1)}, bf16[512]{0:T(512)(128)(2,1)}, u32[]{:S(2)}) copy-start(bf16[512]{0:T(512)(128)(2,1)} %param.27) | copy-start | bytes 3076
  111.0 2.2 %copy-start.3 = (bf16[256,512]{1,0:T(8,128)(2,1)S(1)}, bf16[256,512]{1,0:T(8,128)(2,1)}, u32[]{:S(2)}) copy-start(bf16[256,512]{1,0:T(8,128)(2,1)} %copy-done.2) | copy-start | bytes 786436
Sparse Core Ops, SparseCore 0:
  132.4 10.5 reduce-scatter.1
where the time goes:
time: 152 us; the launch traced here: 150 us
  other arithmetic  48.5 us (32%)
  waiting for transfers between devices  28.3 us (19%)
  matrix products  24.5 us (16%)
  between operations  14.4 us (9%)
  starting transfers between devices  13 us (9%)
  blocking collectives  12.1 us (8%)
  local copies, waits for them, and re-layouts  8.51 us (6%)
    another operation x8, other arithmetic  20.5 us
    ppermute x10, waiting for transfers between devices, shifted(): lax.ppermute(value, axis, [(source, source + steps) for source in range(f...  18.1 us
    reduce_sum x4, other arithmetic, absorb(): weight_mass = weight_mass + jnp.sum(weights, axis=2)  14.7 us
    ppermute x10, starting transfers between devices, shifted(): lax.ppermute(value, axis, [(source, source + steps) for source in range(f...  12.9 us
    reduce_scatter x1, waiting for transfers between devices, local(): lax.psum_scatter((jnp.dot(heads_flat, attend_out, preferred_element_type=...  10.1 us
    psum x1, blocking collectives, local(): center = lax.psum(jnp.sum(filtered, axis=-1), 'tp') / CONV  9.58 us
    dot_general x5, matrix products, project(): jnp.dot(normed, weight, preferred_element_type=jnp.float32)  9.1 us
    dot_general x4, matrix products, absorb(): jnp.einsum('thd,shd->hts', qheads, kblock, preferred_element_type=jnp.flo...  6.78 us
  transfers between devices with their start and end apart: 11, of which 7 were waited for; matrix products, arithmetic and copies ran while one was open for 45% of the time, Pallas kernels for 0%

commit v1 on v0

v1 whole, which is shorter than its diff:
```python
import functools
import math

import jax
import jax.numpy as jnp
from jax import lax
from jax.experimental import pallas as pl
from jax.experimental.pallas import tpu as pltpu
from jax.sharding import PartitionSpec as P

HEAD_DIM = 64
LANES = 128
PAIR = LANES // HEAD_DIM
PACK = 16
SUB = 8
LOG2E = math.log2(math.e)
TOP = 60.0
NEVER = -1e30

rms_eps = 1e-06
norm_eps = 1e-05
mass_floor = 0.01

f32 = jnp.float32
bf16 = jnp.bfloat16


def shifted(value, axis, steps):
    count = lax.axis_size(axis)
    first, last = (max(0, -steps), min(count, count - steps))
    return lax.ppermute(value, axis, [(source, source + steps) for source in range(first, last)])


def turned(value, axis, steps):
    count = lax.axis_size(axis)
    return lax.ppermute(value, axis, [(source, (source + steps) % count) for source in range(count)])


def params(mib=48):
    return pltpu.CompilerParams(vmem_limit_bytes=mib << 20)


def fixed(shape):
    return pl.BlockSpec(shape, lambda *step: (0,) * len(shape))


def cost(flops, size):
    return pl.CostEstimate(flops=int(flops), bytes_accessed=int(size), transcendentals=0)


def query_kernel(x_ref, gain_ref, w_ref, normed_ref, q_ref):
    @pl.when(pl.program_id(0) == 0)
    def _():
        x = x_ref[...].astype(f32)
        scale = lax.rsqrt(jnp.mean(x * x, axis=-1, keepdims=True) + rms_eps)
        normed_ref[...] = (x * scale * gain_ref[...].astype(f32)).astype(bf16)

    q = jnp.dot(normed_ref[...], w_ref[...], preferred_element_type=f32)
    q_ref[...] = (q * (LOG2E * HEAD_DIM ** (-0.5))).astype(bf16)


def project_queries(x, gain, weight):
    rows, width = x.shape
    cols = weight.shape[1]
    tile = min(256, cols)
    return pl.pallas_call(
        query_kernel,
        grid=(cols // tile,),
        in_specs=[fixed((rows, width)), fixed((1, width)), pl.BlockSpec((width, tile), lambda j: (0, j))],
        out_specs=[fixed((rows, width)), pl.BlockSpec((rows, tile), lambda j: (0, j))],
        out_shape=[jax.ShapeDtypeStruct((rows, width), bf16), jax.ShapeDtypeStruct((rows, cols), bf16)],
        compiler_params=params(),
        cost_estimate=cost(2 * rows * width * cols, 2 * width * (2 * rows + cols)),
        name="queries",
    )(x, gain, weight)


def ordering(rows):
    steps = rows // SUB
    place = lax.broadcasted_iota(jnp.int32, (rows, rows), 0)
    key = lax.broadcasted_iota(jnp.int32, (rows, rows), 1)
    return jnp.where((place % SUB) * steps + place // SUB == key, 1.0, 0.0).astype(bf16)


def block_kernel(half, x_ref, wk_ref, wv_ref, off_ref, out_ref, order_ref):
    rows = x_ref.shape[0]
    step = pl.program_id(0)

    @pl.when(step == 0)
    def _():
        order_ref[...] = ordering(rows)

    def put(weight):
        part = jnp.dot(x_ref[...], weight, preferred_element_type=f32).astype(bf16)
        out_ref[:rows, :] = jnp.dot(order_ref[...], part, preferred_element_type=f32).astype(bf16)

    @pl.when(step < half)
    def _():
        put(wk_ref[...])

    @pl.when(step >= half)
    def _():
        put(wv_ref[...])

    out_ref[rows:, :] = off_ref[...]


def project_block(normed, wk, wv, off_rows):
    rows, width = normed.shape
    cols = wk.shape[1]
    tile = min(256, cols)
    half = cols // tile
    extra = off_rows.shape[0]
    return pl.pallas_call(
        functools.partial(block_kernel, half),
        grid=(2 * half,),
        in_specs=[
            fixed((rows, width)),
            pl.BlockSpec((width, tile), lambda j: (0, jnp.minimum(j, half - 1))),
            pl.BlockSpec((width, tile), lambda j: (0, jnp.maximum(j - half, 0))),
            pl.BlockSpec((extra, tile), lambda j: (0, j)),
        ],
        out_specs=pl.BlockSpec((rows + extra, tile), lambda j: (0, j)),
        out_shape=jax.ShapeDtypeStruct((rows + extra, 2 * cols), bf16),
        scratch_shapes=[pltpu.VMEM((rows, rows), bf16)],
        compiler_params=params(),
        cost_estimate=cost(4 * rows * width * cols, 2 * width * (rows + 2 * cols)),
        name="keys_values",
    )(normed, wk, wv, off_rows)


def gate_kernel(x_ref, wi_ref, wg_ref, out_ref):
    values = jnp.dot(x_ref[...], wi_ref[...], preferred_element_type=f32).astype(bf16).astype(f32)
    gates = jnp.dot(x_ref[...], wg_ref[...], preferred_element_type=f32).astype(bf16).astype(f32)
    out_ref[...] = (values * (1.0 / (1.0 + jnp.exp(-gates)))).astype(bf16)


def project_gated(normed, wi, wg):
    rows, width = normed.shape
    cols = wi.shape[1]
    tile = min(256, cols)
    return pl.pallas_call(
        gate_kernel,
        grid=(cols // tile,),
        in_specs=[fixed((rows, width))] + [pl.BlockSpec((width, tile), lambda j: (0, j))] * 2,
        out_specs=pl.BlockSpec((rows, tile), lambda j: (0, j)),
        out_shape=jax.ShapeDtypeStruct((rows, cols), bf16),
        compiler_params=params(),
        cost_estimate=cost(4 * rows * width * cols, 2 * width * (rows + 2 * cols)),
        name="gated",
    )(normed, wi, wg)


def suffix_products(x):
    sub = lax.broadcasted_iota(jnp.int32, x.shape, 0)
    reach = 1
    while reach < SUB:
        x = x * jnp.where(sub < SUB - reach, pltpu.roll(x, SUB - reach, 0), 1.0)
        reach *= 2
    return x, jnp.where(sub < SUB - 1, pltpu.roll(x, SUB - 1, 0), 1.0)


def attend_kernel(causal, has_flag, packed, *refs):
    refs = list(refs)
    flag_ref = refs.pop(0) if has_flag else None
    q_ref = refs.pop(0)
    scores, weights, offs, vt = refs[-4:]
    outs = refs[-5:-4] if packed else refs[-6:-4]
    blocks = refs[: len(refs) - 4 - len(outs)]
    rows, width = q_ref.shape
    heads = width // HEAD_DIM
    steps = rows // SUB
    count = len(blocks)

    for b, block in enumerate(blocks):
        raw = block[rows : rows + PACK, :rows].astype(f32) * LOG2E
        if has_flag and b == count - 1:
            raw = jnp.where(flag_ref[0] > 0, raw, NEVER)
        raw = jnp.concatenate([raw, jnp.zeros((LANES - PACK, rows), f32)], axis=0)
        offs[b] = raw.T
        for p in range(width // LANES):
            v = block[:rows, width + p * LANES : width + (p + 1) * LANES]
            vt[b, p * LANES : (p + 1) * LANES, :] = v.T

    lane = lax.broadcasted_iota(jnp.int32, (rows, LANES), 1) // HEAD_DIM
    totals = []
    for h in range(heads):
        p, inside = h // PAIR, h % PAIR
        cols = slice(p * LANES, (p + 1) * LANES)
        q = jnp.where(lane == inside, q_ref[:, cols], jnp.zeros((), bf16))
        carry = jnp.ones((SUB, rows), f32)
        out = None
        for b, block in enumerate(blocks):
            scores[h % 2, b] = lax.dot_general(
                block[:rows, cols], q, (((1,), (1,)), ((), ())), preferred_element_type=f32
            )
            keep = jnp.ones((SUB, rows), f32)
            parts = [None] * steps
            for t in reversed(range(steps)):
                here = slice(t * SUB, (t + 1) * SUB)
                s = scores[h % 2, b, here, :] + offs[b, here, h : h + 1]
                e = jnp.exp2(jnp.minimum(s, TOP))
                if causal and b == 0:
                    key = lax.broadcasted_iota(jnp.int32, (SUB, rows), 0) * steps + t
                    e = jnp.where(key < lax.broadcasted_iota(jnp.int32, (SUB, rows), 1), e, 0.0)
                keep = keep * (1.0 / (1.0 + e))
                parts[t] = e * keep
            inclusive, exclusive = suffix_products(keep)
            after = exclusive * carry
            carry = carry * jnp.broadcast_to(inclusive[:1], (SUB, rows))
            for t in range(0, steps, 2):
                pair = jnp.concatenate([parts[t] * after, parts[t + 1] * after], axis=0)
                weights[h % 2, b, t * SUB : (t + 2) * SUB, :] = pair.astype(bf16)
            part = jnp.dot(
                vt[b, h * HEAD_DIM : (h + 1) * HEAD_DIM, :], weights[h % 2, b], preferred_element_type=f32
            )
            out = part if out is None else out + part
        totals.append(carry[:1])
        outs[0][h * HEAD_DIM : (h + 1) * HEAD_DIM, :] = out.astype(outs[0].dtype)

    rest = jnp.concatenate(totals, axis=0)
    if packed:
        mass = 1.0 - rest
        high = mass.astype(bf16)
        low = (mass - high.astype(f32)).astype(bf16)
        fill = outs[0].shape[0] - width - 2 * heads
        stats = [high.astype(f32), low.astype(f32)]
        if fill:
            stats.append(jnp.zeros((fill, rows), f32))
        outs[0][width:, :] = jnp.concatenate(stats, axis=0).astype(bf16)
    else:
        outs[1][...] = rest


def stat_rows(heads):
    return -(-2 * heads // PACK) * PACK


def attend(q, blocks, flag, causal, packed, name):
    rows, width = q.shape
    heads = width // HEAD_DIM
    count = len(blocks)
    if packed:
        out_shape = [jax.ShapeDtypeStruct((width + stat_rows(heads), rows), bf16)]
    else:
        out_shape = [jax.ShapeDtypeStruct((width, rows), f32), jax.ShapeDtypeStruct((heads, rows), f32)]
    whole = pl.BlockSpec(memory_space=pltpu.VMEM)
    args = ([] if flag is None else [flag]) + [q] + list(blocks)
    specs = ([] if flag is None else [pl.BlockSpec(memory_space=pltpu.SMEM)]) + [whole] * (1 + count)
    out = pl.pallas_call(
        functools.partial(attend_kernel, causal, flag is not None, packed),
        in_specs=specs,
        out_specs=[whole] * len(out_shape),
        out_shape=out_shape,
        scratch_shapes=[
            pltpu.VMEM((2, count, rows, rows), f32),
            pltpu.VMEM((2, count, rows, rows), bf16),
            pltpu.VMEM((count, rows, LANES), f32),
            pltpu.VMEM((count, width, rows), bf16),
        ],
        compiler_params=params(),
        cost_estimate=cost(600 * count * rows * rows * heads, 2 * rows * width * (2 + 2 * count)),
        name=name,
    )(*args)
    return out[0] if packed else out


def output_kernel(visits, me_ref, *refs):
    attA, restA, attC, restC = refs[:4]
    results = refs[4 : 4 + visits]
    gain_ref, conv_ref, wa_ref, wf_ref, out_ref, mass_ref, heads_ref, heads_bf = refs[4 + visits :]
    width, rows = attA.shape
    heads = width // HEAD_DIM
    shares = out_ref.shape[0]
    chunk = rows // shares

    @pl.when(pl.program_id(0) == 0)
    def _():
        rest = restA[...]
        scales = [rest]
        rest = rest * restC[...]
        for result in results:
            scales.append(rest)
            high = result[width : width + heads, :].astype(f32)
            low = result[width + heads : width + 2 * heads, :].astype(f32)
            rest = rest * (1.0 - (high + low))
        mass_ref[...] = jnp.log(jnp.maximum(1.0 - rest, mass_floor))
        for h in range(heads):
            mine = slice(h * HEAD_DIM, (h + 1) * HEAD_DIM)
            total = attA[mine, :] + scales[0][h : h + 1] * attC[mine, :]
            for result, scale in zip(results, scales[1:]):
                total = total + scale[h : h + 1] * result[mine, :].astype(f32)
            norm = lax.rsqrt(jnp.mean(total * total, axis=0, keepdims=True) + rms_eps)
            heads_ref[mine, :] = total * norm
        for p in range(width // LANES):
            cols = slice(p * LANES, (p + 1) * LANES)
            both = heads_ref[cols, :].T * gain_ref[:, cols].astype(f32)
            heads_bf[:, cols] = both.astype(bf16)

    me = me_ref[0]
    for t in range(shares):
        place = lax.rem(me + t, shares) * chunk
        mine = pl.ds(pl.multiple_of(place, chunk), chunk)
        got = jnp.dot(heads_bf[mine, :], wa_ref[...], preferred_element_type=f32)
        got = got + jnp.dot(conv_ref[mine, :], wf_ref[...], preferred_element_type=f32)
        out_ref[t] = got.astype(bf16)


def project_out(me, shares, attA, restA, attC, restC, results, gain, conv_out, wa, wf):
    width, rows = attA.shape
    heads = width // HEAD_DIM
    depth = wa.shape[1]
    tile = min(512, depth)

    return pl.pallas_call(
        functools.partial(output_kernel, len(results)),
        grid=(depth // tile,),
        in_specs=[pl.BlockSpec(memory_space=pltpu.SMEM)]
        + [fixed(a.shape) for a in (attA, restA, attC, restC, *results, gain, conv_out)]
        + [pl.BlockSpec((width, tile), lambda j: (0, j))] * 2,
        out_specs=[pl.BlockSpec((shares, rows // shares, tile), lambda j: (0, 0, j)), fixed((heads, rows))],
        out_shape=[
            jax.ShapeDtypeStruct((shares, rows // shares, depth), bf16),
            jax.ShapeDtypeStruct((heads, rows), f32),
        ],
        scratch_shapes=[pltpu.VMEM((width, rows), f32), pltpu.VMEM((rows, width), bf16)],
        compiler_params=params(),
        cost_estimate=cost(4 * rows * width * depth, 4 * width * depth),
        name="output",
    )(me, attA, restA, attC, restC, *results, gain, conv_out, wa, wf)


def local(
    stream,
    norm_gain,
    query_weight,
    key_weight,
    value_weight,
    filter_input,
    filter_gate,
    score_offset,
    head_gain,
    filter_taps,
    channel_gain,
    channel_shift,
    attend_out,
    filter_out,
):
    rows = stream.shape[1]
    width = query_weight.shape[1]
    heads = width // HEAD_DIM
    ring = lax.axis_size("sp")
    shares = lax.axis_size("tp")
    channels = filter_taps.shape[1] * shares

    normed, queries = project_queries(stream[0], norm_gain[None], query_weight)
    visiting = [shifted(queries, "sp", -2 * s) for s in range(1, (ring + 1) // 2)]

    off = score_offset[0].reshape(SUB, rows // SUB, heads).transpose(2, 1, 0).reshape(heads, rows)
    off = jnp.pad(off, ((0, -heads % PACK), (0, 2 * width - rows)))
    block = project_block(normed, key_weight, value_weight, off)
    block_before = shifted(block, "sp", 1)
    flag = (lax.axis_index("sp") > 0).astype(jnp.int32)[None]

    gated = project_gated(normed, filter_input, filter_gate)
    reach_back = filter_taps.shape[0] - 1
    earlier = shifted(gated[rows - reach_back :], "sp", 1)

    attA, restA = attend(queries, [block], None, True, False, "attend_own")
    results = []
    for s, visitor in enumerate(visiting):
        result = attend(visitor, [block, block_before], flag, False, True, "attend_visitor")
        results.append(shifted(result, "sp", 2 * (s + 1)))
    attC, restC = attend(queries, [block_before], flag, False, False, "attend_before")

    extended = jnp.concatenate([earlier, gated], axis=0).astype(f32)
    tap_values = filter_taps.astype(f32)
    filtered = jnp.zeros((rows, gated.shape[1]), f32)
    for tap_index in range(reach_back + 1):
        filtered = filtered + extended[tap_index : tap_index + rows] * tap_values[tap_index]
    here = filtered.shape[1]
    own_sum = jnp.sum(filtered, axis=-1)
    own_dev = filtered - (own_sum / here)[:, None]
    own_stats = jnp.stack([own_sum, jnp.sum(own_dev * own_dev, axis=-1)])
    stats = [own_stats] + [turned(own_stats, "tp", t) for t in range(1, shares)]
    center = sum(s[0] for s in stats) / channels
    spread = sum(s[1] + here * (s[0] / here - center) ** 2 for s in stats) / channels
    conv_out = jax.nn.silu(
        (filtered - center[:, None]) * lax.rsqrt(spread[:, None] + norm_eps) * channel_gain.astype(f32)
        + channel_shift.astype(f32)
    ).astype(bf16)

    me = lax.axis_index("tp").astype(jnp.int32)[None]
    out, mass = project_out(
        me, shares, attA, restA, attC, restC, results, head_gain[None], conv_out, attend_out, filter_out
    )
    total = out[0].astype(f32)
    for t in range(1, shares):
        total = total + turned(out[t], "tp", t).astype(f32)
    return (total.astype(bf16)[None], mass.T[None])


def solution(mesh):
    return jax.shard_map(
        local,
        mesh=mesh,
        in_specs=(
            P("fs", "sp", None),
            P(),
            P(None, "tp"),
            P(None, "tp"),
            P(None, "tp"),
            P(None, "tp"),
            P(None, "tp"),
            P("fs", "sp", "tp"),
            P("tp"),
            P(None, "tp"),
            P("tp"),
            P("tp"),
            P("tp", None),
            P("tp", None),
        ),
        out_specs=(P("fs", ("sp", "tp"), None), P("fs", "sp", "tp")),
        check_vma=False,
    )
```

time: 152 us -> 62.4 us (0.41); the launches traced: 150 us -> 62 us
  other arithmetic: 48.5 us -> 4.08 us
  matrix products: 24.5 us -> 0 us
  Pallas kernels: 0 us -> 24.2 us
  waiting for transfers between devices: 28.3 us -> 11.9 us
  between operations: 14.4 us -> 0.92 us
  blocking collectives: 12.1 us -> 0 us
    dot_general x15 -> x0, matrix products: 24.5 us -> none  [the longest x5 9.1 us: project(): jnp.dot(normed, weight, preferred_element_type=jnp.float32)]
    pallas_call x0 -> x7, Pallas kernels: none -> 24.2 us  [the longest x3 11.9 us: attend(): pl.pallas_call(functools.partial(attend_kernel, causal, flag is not None,...]
    reduce_sum x12 -> x2, other arithmetic: 25.3 us -> 2.79 us  [the longest x1 2.59 us: local(): own_sum = jnp.sum(filtered, axis=-1)]
    another operation x12 -> x1, other arithmetic: 21 us -> 0.01 us  [local(): own_stats = jnp.stack([own_sum, jnp.sum(own_dev * own_dev, axis=-1)])]
    psum x2 -> x0, blocking collectives: 12.1 us -> none  [the longest x1 9.58 us: local(): center = lax.psum(jnp.sum(filtered, axis=-1), 'tp') / CONV]
    reduce_scatter x1 -> x0, waiting for transfers between devices: 10.1 us -> none  [local(): lax.psum_scatter((jnp.dot(heads_flat, attend_out, preferred_element_type=...]
    ppermute x10 -> x4, waiting for transfers between devices: 18.1 us -> 10.3 us  [shifted(): lax.ppermute(value, axis, [(source, source + steps) for source in range(f...]
    unnamed x21 -> x24, local copies, waits for them, and re-layouts: 1.6 us -> 6.03 us
  transfers between devices with their start and end apart: 11 -> 6, of which waited for: 7 -> 3; matrix products, arithmetic and copies ran while one was open for 45% -> 6% of each run, Pallas kernels for 0% -> 18%
where the time goes in v1:
time: 62.4 us; the launch traced here: 62 us
  Pallas kernels  24.2 us (39%)
  starting transfers between devices  13.7 us (22%)
  waiting for transfers between devices  11.9 us (19%)
  local copies, waits for them, and re-layouts  7.17 us (11%)
  other arithmetic  4.08 us (7%)
  between operations  0.92 us (1%)
    pallas_call x3, Pallas kernels, attend(): pl.pallas_call(functools.partial(attend_kernel, causal, flag is not None,...  11.9 us
    ppermute x4, waiting for transfers between devices, shifted(): lax.ppermute(value, axis, [(source, source + steps) for source in range(f...  10.3 us
    ppermute x4, starting transfers between devices, shifted(): lax.ppermute(value, axis, [(source, source + steps) for source in range(f...  9.85 us
    unnamed x24, local copies, waits for them, and re-layouts  6.03 us
    pallas_call x1, Pallas kernels, project_out(): pl.pallas_call(functools.partial(output_kernel, len(results)), grid=(dept...  4.52 us
    ppermute x2, starting transfers between devices, turned(): lax.ppermute(value, axis, [(source, (source + steps) % count) for source...  3.88 us
    pallas_call x1, Pallas kernels, project_block(): pl.pallas_call(functools.partial(block_kernel, half), grid=(2 * half,), i...  3.8 us
    reduce_sum x1, other arithmetic, local(): own_sum = jnp.sum(filtered, axis=-1)  2.59 us
  transfers between devices with their start and end apart: 6, of which 3 were waited for; matrix products, arithmetic and copies ran while one was open for 6% of the time, Pallas kernels for 18%

profile of v1, /device:TPU:27, one launch (start us, length us, event | category | flops | bytes accessed | tf_op | source)
XLA Modules:
  0.0 62.0 jit_solution(15486412282497182099)
XLA Ops:
  0.6 0.7 %broadcast_in_dim.26.gain_ref = bf16[1,2048]{1,0:T(2,128)(2,1)S(1)} reshape(bf16[2048]{0:T(1024)(128)(2,1)} %param.15) | data formatting | bytes 8192 | tf_op jit(solution)/shard_map/broadcast_in_dim | solution.py:356
  1.3 0.0 copy-start
  1.3 1.6 %copy-done = bf16[2048,512]{1,0:T(8,128)(2,1)S(1)} copy-done((bf16[2048,512]{1,0:T(8,128)(2,1)S(1)}, bf16[2048,512]{1,0:T(8,128)(2,1)}, u32[]{:S(2)}) %copy-start) | copy-done | bytes 2097176
  2.9 0.0 copy-start.6
  2.9 1.2 %copy-done.6 = bf16[1,256,2048]{2,1,0:T(8,128)(2,1)S(1)} copy-done((bf16[1,256,2048]{2,1,0:T(8,128)(2,1)S(1)}, bf16[1,256,2048]{2,1,0:T(8,128)(2,1)}, u32[]{:S(2)}) %copy-start.6) | copy-done | bytes 1048600
  4.1 0.0 copy-start.1
  4.1 2.1 %queries.1 = (bf16[256,2048]{1,0:T(8,128)(2,1)S(1)}, bf16[256,512]{1,0:T(8,128)(2,1)}) custom-call(bf16[256,2048]{1,0:T(8,128)(2,1)S(1)} %bitcast.51, bf16[1,2048]{1,0:T(2,128)(2,1)S(1)} %broadcast_in_dim.26.gain_ref, bf16[2048,512]{1,0:T(8,128)(2,1)S(1)} %copy-done), custom_call_target="tpu_custom_call" | custom-call | flops 536870912 | bytes 4194304 | tf_op jit(solution)/shard_map/queries/pallas_call | solution.py:66
  6.3 0.0 copy-done.1
  6.3 0.0 copy-start.2
  6.3 1.6 %copy-done.2 = bf16[2048,512]{1,0:T(8,128)(2,1)S(1)} copy-done((bf16[2048,512]{1,0:T(8,128)(2,1)S(1)}, bf16[2048,512]{1,0:T(8,128)(2,1)}, u32[]{:S(2)}) %copy-start.2) | copy-done | bytes 2097176
  7.9 0.0 copy-start.8
  7.9 0.0 copy-start.3
  7.9 1.8 %gated.1 = bf16[256,512]{1,0:T(8,128)(2,1)S(1)} custom-call(bf16[256,2048]{1,0:T(8,128)(2,1)S(1)} %get-tuple-element.11.x_ref, bf16[2048,512]{1,0:T(8,128)(2,1)S(1)} %copy-done.1, bf16[2048,512]{1,0:T(8,128)(2,1)S(1)} %copy-done.2), custom_call_target="tpu_custom_call" | custom-call | flops 1073741824 | bytes 5242880 | tf_op jit(solution)/shard_map/gated/pallas_call | solution.py:142
  9.7 1.3 %collective-permute-start.3 = (bf16[30,512]{1,0:T(8,128)(2,1)S(1)}, bf16[30,512]{1,0:T(8,128)(2,1)S(1)}, u32[]{:S(2)}, u32[]{:S(2)}) collective-permute-start(bf16[30,512]{1,0:T(8,128)(2,1)S(1)} %slice.269), channel_id=1, source_target_pairs={{0,8},{8,16},{16,24},{1,9},{9,17},{17,25},{2,10},{10,18},{18,26},{... | collective-permute-start | bytes 92168 | tf_op jit(solution)/shard_map/ppermute | solution.py:31
  11.0 0.0 copy-done.8
  11.0 0.1 reshape_squeeze.3
  11.1 0.1 copy.17
  11.2 0.1 reshape.51
  11.3 0.0 copy-done.3
  11.4 0.0 copy-start.4
  11.4 1.6 %copy-done.4 = bf16[2048,512]{1,0:T(8,128)(2,1)S(1)} copy-done((bf16[2048,512]{1,0:T(8,128)(2,1)S(1)}, bf16[2048,512]{1,0:T(8,128)(2,1)}, u32[]{:S(2)}) %copy-start.4) | copy-done | bytes 2097176
  12.9 0.0 copy-start.7
  13.0 3.8 %keys_values.1.refs_1_.refs_2_ = bf16[272,1024]{1,0:T(8,128)(2,1)} custom-call(bf16[256,2048]{1,0:T(8,128)(2,1)S(1)} %get-tuple-element.11.x_ref, bf16[2048,512]{1,0:T(8,128)(2,1)S(1)} %copy-done.3, bf16[2048,512]{1,0:T(8,128)(2,1)S(1)} %copy-done.4, bf16[16,1024]{1,0:T(8,128)(2,1)S(1)} %pad.4.off_ref), custom_call_target="tpu_custom_call" | custom-call | flops 1073741824 | bytes 5242880 | tf_op jit(solution)/shard_map/keys_values/pallas_call | solution.py:114
  16.8 1.3 %collective-permute-start = (bf16[272,1024]{1,0:T(8,128)(2,1)}, bf16[272,1024]{1,0:T(8,128)(2,1)S(1)}, u32[]{:S(2)}, u32[]{:S(2)}) collective-permute-start(bf16[272,1024]{1,0:T(8,128)(2,1)} %keys_values.1.refs_1_.refs_2_), channel_id=1, source_target_pairs={{0,8},{8,16},{16,24},{1,9},{9,17},{17,25},{2,10},{10,18},{18,26},{... | collective-permute-start | bytes 1671176 | tf_op jit(solution)/shard_map/ppermute | solution.py:31
  18.0 5.8 %collective-permute-start.1 = (bf16[256,512]{1,0:T(8,128)(2,1)}, bf16[256,512]{1,0:T(8,128)(2,1)S(1)}, u32[]{:S(2)}, u32[]{:S(2)}) collective-permute-start(bf16[256,512]{1,0:T(8,128)(2,1)} %get-tuple-element.10.refs_0_.refs_1_), channel_id=1, source_target_pairs={{16,0},{24,8},{17,1},{25,9},{18,2},{26,10},{19,3},{27,11},{20,4},{... | collective-permute-start | bytes 786440 | tf_op jit(solution)/shard_map/ppermute | solution.py:31
  23.9 0.0 copy-done.7
  23.9 0.0 collective-permute-done.3
  23.9 0.1 maximum_convert_fusion
  24.0 0.0 copy-start.9
  24.0 0.0 copy-start.10
  24.1 0.0 copy-start.11
  24.1 2.6 %fusion.32 = (f32[256]{0:T(256)S(1)}, f32[256,512]{1,0:T(8,128)S(1)}) fusion(f32[512]{0:T(512)S(1)} %bitcast.85, f32[286,512]{1,0:T(8,128)S(1)} %maximum_convert_fusion, f32[512]{0:T(512)S(1)} %bitcast.84, f32[512]{0:T(512)S(1)} %bitcast.83, f32[512]{0:T(512)S(1)} %bitcast.82, f32[512]{0:T(512)S(1)} %bitcast.81, f32[512]{0:T(512)S(1)} %bitcast.80, ...), kind=kLoop, calls=%fused_computation.72 | loop fusion | flops 8126208 | bytes 16841728 | tf_op jit(solution)/shard_map/reduce_sum | solution.py:382
  26.7 0.2 multiply_reduce_fusion
  26.9 1.6 %collective-permute-start.4 = (f32[2,256]{1,0:T(2,128)S(1)}, f32[2,256]{1,0:T(2,128)S(1)}, u32[]{:S(2)}, u32[]{:S(2)}) collective-permute-start(f32[2,256]{1,0:T(2,128)S(1)} %pad_maximum_fusion), channel_id=1, source_target_pairs={{0,1},{1,0},{2,3},{3,2},{4,5},{5,4},{6,7},{7,6},{8,9},{9,8},{10,11... | collective-permute-start | bytes 6152 | tf_op jit(solution)/shard_map/ppermute | solution.py:36
  28.5 3.9 %attend_own.1 = (f32[512,256]{1,0:T(8,128)S(1)}, f32[8,256]{1,0:T(8,128)S(1)}) custom-call(bf16[256,512]{1,0:T(8,128)(2,1)} %get-tuple-element.10.refs_0_.refs_1_, bf16[272,1024]{1,0:T(8,128)(2,1)} %keys_values.1.refs_1_.refs_2_), custom_call_target="tpu_custom_call" | custom-call | flops 314572800 | bytes 1048576 | tf_op jit(solution)/shard_map/attend_own/pallas_call | solution.py:250
  32.4 0.0 copy-done.9
  32.4 0.0 copy-done.10
  32.4 0.0 copy-done.11
  32.4 0.0 collective-permute-done.4
  32.5 0.0 collective-permute-done.1.refs_1_
  32.5 0.5 collective-permute-done.refs_2_.refs_3_
  33.0 0.0 copy-start.5
  33.0 4.4 %attend_visitor.1 = bf16[528,256]{1,0:T(8,128)(2,1)S(1)} custom-call(s32[1]{0:T(128)} %bitcast.3.refs_0_, bf16[256,512]{1,0:T(8,128)(2,1)S(1)} %collective-permute-done.1.refs_1_, bf16[272,1024]{1,0:T(8,128)(2,1)} %keys_values.1.refs_1_.refs_2_, bf16[272,1024]{1,0:T(8,128)(2,1)S(1)} %collective-permute-done.refs_2_.refs_3_), custom_call_target="tpu_custom_call" | custom-call | flops 629145600 | bytes 1572864 | tf_op jit(solution)/shard_map/attend_visitor/pallas_call | solution.py:250
  37.4 1.5 %collective-permute-start.2 = (bf16[528,256]{1,0:T(8,128)(2,1)S(1)}, bf16[528,256]{1,0:T(8,128)(2,1)S(1)}, u32[]{:S(2)}, u32[]{:S(2)}) collective-permute-start(bf16[528,256]{1,0:T(8,128)(2,1)S(1)} %attend_visitor.1), channel_id=1, source_target_pairs={{0,16},{8,24},{1,17},{9,25},{2,18},{10,26},{3,19},{11,27},{4,20},{... | collective-permute-start | bytes 811016 | tf_op jit(solution)/shard_map/ppermute | solution.py:31
  38.9 0.3 multiply_convert_fusion.refs_6_
  39.1 3.7 %attend_before.1 = (f32[512,256]{1,0:T(8,128)S(1)}, f32[8,256]{1,0:T(8,128)S(1)}) custom-call(s32[1]{0:T(128)} %bitcast.3.refs_0_, bf16[256,512]{1,0:T(8,128)(2,1)} %get-tuple-element.10.refs_0_.refs_1_, bf16[272,1024]{1,0:T(8,128)(2,1)S(1)} %collective-permute-done.refs_2_.refs_3_), custom_call_target="tpu_custom_call" | custom-call | flops 314572800 | bytes 1048576 | tf_op jit(solution)/shard_map/attend_before/pallas_call | solution.py:250
  42.8 9.8 %collective-permute-done.2.refs_4_ = bf16[528,256]{1,0:T(8,128)(2,1)S(1)} collective-permute-done((bf16[528,256]{1,0:T(8,128)(2,1)S(1)}, bf16[528,256]{1,0:T(8,128)(2,1)S(1)}, u32[]{:S(2)}, u32[]{:S(2)}) %collective-permute-start.2) | collective-permute-done | bytes 270368 | tf_op jit(solution)/shard_map/ppermute | solution.py:31
  52.6 0.0 copy-done.5
  52.6 4.5 %output.1 = (bf16[2,128,2048]{2,1,0:T(8,128)(2,1)S(1)}, f32[8,256]{1,0:T(8,128)}) custom-call(s32[1]{0:T(128)} %bitcast.me_ref, f32[512,256]{1,0:T(8,128)S(1)} %get-tuple-element.12.refs_0_, f32[8,256]{1,0:T(8,128)S(1)} %get-tuple-element.13.refs_1_, f32[512,256]{1,0:T(8,128)S(1)} %get-tuple-element.14.refs_2_, f32[8,256]{1,0:T(8,128)S(1)} %get-tuple-element.15.refs_3_, ...), custom_call_target="tpu_custom_call" | custom-call | flops 1073741824 | bytes 4194304 | tf_op jit(solution)/shard_map/output/pallas_call | solution.py:315
  57.2 2.3 %collective-permute-start.5 = (bf16[128,2048]{1,0:T(8,128)(2,1)S(1)}, bf16[128,2048]{1,0:T(8,128)(2,1)S(1)}, u32[]{:S(2)}, u32[]{:S(2)}) collective-permute-start(bf16[128,2048]{1,0:T(8,128)(2,1)S(1)} %slice_bitcast_fusion), channel_id=1, source_target_pairs={{0,1},{1,0},{2,3},{3,2},{4,5},{5,4},{6,7},{7,6},{8,9},{9,8},{10,11... | collective-permute-start | bytes 1572872 | tf_op jit(solution)/shard_map/ppermute | solution.py:36
  59.5 1.5 %collective-permute-done.5 = bf16[128,2048]{1,0:T(8,128)(2,1)S(1)} collective-permute-done((bf16[128,2048]{1,0:T(8,128)(2,1)S(1)}, bf16[128,2048]{1,0:T(8,128)(2,1)S(1)}, u32[]{:S(2)}, u32[]{:S(2)}) %collective-permute-start.5) | collective-permute-done | bytes 524320 | tf_op jit(solution)/shard_map/ppermute | solution.py:36
  61.0 0.9 %fusion.1 = bf16[1,128,2048]{2,1,0:T(8,128)(2,1)} fusion(bf16[128,2048]{1,0:T(8,128)(2,1)S(1)} %collective-permute-done.5, bf16[2,128,2048]{2,1,0:T(8,128)(2,1)S(1)} %get-tuple-element.16), kind=kLoop, calls=%fused_computation.2 | loop fusion | flops 1048576 | bytes 1572864 | tf_op jit(solution)/shard_map/broadcast_in_dim | solution.py:400
  (12 shorter events, 0.2 us)
Async XLA Ops:
  1.3 1.6 %copy-start = (bf16[2048,512]{1,0:T(8,128)(2,1)S(1)}, bf16[2048,512]{1,0:T(8,128)(2,1)}, u32[]{:S(2)}) copy-start(bf16[2048,512]{1,0:T(8,128)(2,1)} %w_ref.1) | copy-start | bytes 6291460
  2.9 1.2 %copy-start.6 = (bf16[1,256,2048]{2,1,0:T(8,128)(2,1)S(1)}, bf16[1,256,2048]{2,1,0:T(8,128)(2,1)}, u32[]{:S(2)}) copy-start(bf16[1,256,2048]{2,1,0:T(8,128)(2,1)} %param.14) | copy-start | bytes 3145732
  4.1 2.1 %copy-start.1 = (bf16[2048,512]{1,0:T(8,128)(2,1)S(1)}, bf16[2048,512]{1,0:T(8,128)(2,1)}, u32[]{:S(2)}) copy-start(bf16[2048,512]{1,0:T(8,128)(2,1)} %wi_ref.1) | copy-start | bytes 6291460
  6.3 1.6 %copy-start.2 = (bf16[2048,512]{1,0:T(8,128)(2,1)S(1)}, bf16[2048,512]{1,0:T(8,128)(2,1)}, u32[]{:S(2)}) copy-start(bf16[2048,512]{1,0:T(8,128)(2,1)} %wg_ref.1) | copy-start | bytes 6291460
  7.9 3.1 %copy-start.8 = (bf16[1,256,8]{1,2,0:T(8,128)(2,1)S(1)}, bf16[1,256,8]{1,2,0:T(8,128)(2,1)}, u32[]{:S(2)}) copy-start(bf16[1,256,8]{1,2,0:T(8,128)(2,1)} %param.21) | copy-start | bytes 12292
  7.9 3.5 %copy-start.3 = (bf16[2048,512]{1,0:T(8,128)(2,1)S(1)}, bf16[2048,512]{1,0:T(8,128)(2,1)}, u32[]{:S(2)}) copy-start(bf16[2048,512]{1,0:T(8,128)(2,1)} %wk_ref.1) | copy-start | bytes 6291460
  9.7 14.2 %collective-permute-start.3 = (bf16[30,512]{1,0:T(8,128)(2,1)S(1)}, bf16[30,512]{1,0:T(8,128)(2,1)S(1)}, u32[]{:S(2)}, u32[]{:S(2)}) collective-permute-start(bf16[30,512]{1,0:T(8,128)(2,1)S(1)} %slice.269), channel_id=1, source_target_pairs={{0,8},{8,16},{16,24},{1,9},{9,17},{17,25},{2,10},{10,18},{18,26},{... | collective-permute-start | bytes 92168 | tf_op jit(solution)/shard_map/ppermute | solution.py:31
  11.4 1.6 %copy-start.4 = (bf16[2048,512]{1,0:T(8,128)(2,1)S(1)}, bf16[2048,512]{1,0:T(8,128)(2,1)}, u32[]{:S(2)}) copy-start(bf16[2048,512]{1,0:T(8,128)(2,1)} %wv_ref.1) | copy-start | bytes 6291460
  12.9 10.9 %copy-start.7 = (bf16[31,512]{1,0:T(8,128)(2,1)S(1)}, bf16[31,512]{1,0:T(8,128)(2,1)}, u32[]{:S(2)}) copy-start(bf16[31,512]{1,0:T(8,128)(2,1)} %param.23) | copy-start | bytes 95236
  16.8 16.2 %collective-permute-start = (bf16[272,1024]{1,0:T(8,128)(2,1)}, bf16[272,1024]{1,0:T(8,128)(2,1)S(1)}, u32[]{:S(2)}, u32[]{:S(2)}) collective-permute-start(bf16[272,1024]{1,0:T(8,128)(2,1)} %keys_values.1.refs_1_.refs_2_), channel_id=1, source_target_pairs={{0,8},{8,16},{16,24},{1,9},{9,17},{17,25},{2,10},{10,18},{18,26},{... | collective-permute-start | bytes 1671176 | tf_op jit(solution)/shard_map/ppermute | solution.py:31
  18.0 14.4 %collective-permute-start.1 = (bf16[256,512]{1,0:T(8,128)(2,1)}, bf16[256,512]{1,0:T(8,128)(2,1)S(1)}, u32[]{:S(2)}, u32[]{:S(2)}) collective-permute-start(bf16[256,512]{1,0:T(8,128)(2,1)} %get-tuple-element.10.refs_0_.refs_1_), channel_id=1, source_target_pairs={{16,0},{24,8},{17,1},{25,9},{18,2},{26,10},{19,3},{27,11},{20,4},{... | collective-permute-start | bytes 786440 | tf_op jit(solution)/shard_map/ppermute | solution.py:31
  24.0 8.3 %copy-start.9 = (bf16[512]{0:T(512)(128)(2,1)S(1)}, bf16[512]{0:T(512)(128)(2,1)}, u32[]{:S(2)}) copy-start(bf16[512]{0:T(512)(128)(2,1)} %param.24) | copy-start | bytes 3076
  24.0 8.4 %copy-start.10 = (bf16[512]{0:T(512)(128)(2,1)S(1)}, bf16[512]{0:T(512)(128)(2,1)}, u32[]{:S(2)}) copy-start(bf16[512]{0:T(512)(128)(2,1)} %param.25) | copy-start | bytes 3076
  24.1 8.4 %copy-start.11 = (bf16[512]{0:T(512)(128)(2,1)S(1)}, bf16[512]{0:T(512)(128)(2,1)}, u32[]{:S(2)}) copy-start(bf16[512]{0:T(512)(128)(2,1)} %param.22) | copy-start | bytes 3076
  26.9 5.6 %collective-permute-start.4 = (f32[2,256]{1,0:T(2,128)S(1)}, f32[2,256]{1,0:T(2,128)S(1)}, u32[]{:S(2)}, u32[]{:S(2)}) collective-permute-start(f32[2,256]{1,0:T(2,128)S(1)} %pad_maximum_fusion), channel_id=1, source_target_pairs={{0,1},{1,0},{2,3},{3,2},{4,5},{5,4},{6,7},{7,6},{8,9},{9,8},{10,11... | collective-permute-start | bytes 6152 | tf_op jit(solution)/shard_map/ppermute | solution.py:36
  33.0 19.6 %copy-start.5 = (bf16[512,2048]{1,0:T(8,128)(2,1)S(1)}, bf16[512,2048]{1,0:T(8,128)(2,1)}, u32[]{:S(2)}) copy-start(bf16[512,2048]{1,0:T(8,128)(2,1)} %refs_7_.1) | copy-start | bytes 6291460
  37.4 15.2 %collective-permute-start.2 = (bf16[528,256]{1,0:T(8,128)(2,1)S(1)}, bf16[528,256]{1,0:T(8,128)(2,1)S(1)}, u32[]{:S(2)}, u32[]{:S(2)}) collective-permute-start(bf16[528,256]{1,0:T(8,128)(2,1)S(1)} %attend_visitor.1), channel_id=1, source_target_pairs={{0,16},{8,24},{1,17},{9,25},{2,18},{10,26},{3,19},{11,27},{4,20},{... | collective-permute-start | bytes 811016 | tf_op jit(solution)/shard_map/ppermute | solution.py:31
  57.2 3.8 %collective-permute-start.5 = (bf16[128,2048]{1,0:T(8,128)(2,1)S(1)}, bf16[128,2048]{1,0:T(8,128)(2,1)S(1)}, u32[]{:S(2)}, u32[]{:S(2)}) collective-permute-start(bf16[128,2048]{1,0:T(8,128)(2,1)S(1)} %slice_bitcast_fusion), channel_id=1, source_target_pairs={{0,1},{1,0},{2,3},{3,2},{4,5},{5,4},{6,7},{7,6},{8,9},{9,8},{10,11... | collective-permute-start | bytes 1572872 | tf_op jit(solution)/shard_map/ppermute | solution.py:36
